TPU v7x, 32 devices: a whole 2x2x4 slice. The times are simulated.
32 devices in a mesh: grp: 2 (over y), ep: 8 (over z, x), tp: 2 (over core).
Axes of the slice: x: 2, y: 2, z: 4, core: 2. Of those that a mesh axis runs over, the one named last changes fastest.
Arguments:
- tokens: bfloat16 [4096, 2048], P(('grp', 'ep'), 'tp'), parts along dimension 0, may hold values from -6 to 6
- norm_gain: bfloat16 [2048], P('tp'), may hold values from 0.099609375 to 1.8984375
- w_gate: bfloat16 [8, 2048, 1024], P('ep', None, 'tp'), may hold values from -0.125 to 0.125
- w_up: bfloat16 [8, 2048, 1024], P('ep', None, 'tp'), may hold values from -0.125 to 0.125
- w_down: bfloat16 [8, 1024, 2048], P('ep', 'tp'), may hold values from -0.1875 to 0.1875
- expert_ids: int32 [4096, 2], P(('grp', 'ep')), parts along dimension 0, may hold values from 0 to 7, as said below
- combine: float32 [4096, 2], P(('grp', 'ep')), parts along dimension 0, may hold values from 0.1 to 1
- final_gain: bfloat16 [2048], P('tp'), may hold values from 0.099609375 to 1.8984375
Outputs:
- result: bfloat16 [4096, 2048], P(('grp', 'ep'), 'tp'), parts along dimension 0
There are 2 independent parts, one for each index of `grp`. A program takes and returns all parts, laid end to end along the dimension named above; an argument that names none is the same for every part. Nothing has to cross between parts.
Inputs may be any that keep to these rules, and one draw needn't show every extreme that they name: `expert_ids`: the experts form 4 groups of consecutive ids of equal size; the 2 experts of a row are different and lie in one group. Among the rows of one index of ep no expert is named more than 160 times, and in each such block some expert is named exactly 160 times.
All inputs are finite; a program needn't handle non-finite values.
Results may differ from a plain program's by a relative error of at most 0.0077.
Values may be sent and summed in bfloat16 or wider, within the bound.
A program may use at most 64 MiB of HBM per device.

v0:
```python
import jax
import jax.numpy as jnp
from jax import lax
from jax.sharding import PartitionSpec as P

GROUPS = 4


def body(tokens, norm_gain, w_gate, w_up, w_down, expert_ids, combine, final_gain):
    eps = 1e-06
    tok_dev, half = tokens.shape
    n_ep = lax.axis_size("ep")
    n_tp = lax.axis_size("tp")
    width = half * n_tp
    exp_dev = w_gate.shape[0]
    experts = exp_dev * n_ep
    per_group = experts // GROUPS
    capacity = tok_dev // 8 * 5 * 2 // per_group
    top = expert_ids.shape[1]
    narrow = tokens.astype(jnp.float32)
    squares = lax.psum(jnp.sum(narrow * narrow, axis=1), "tp")
    scale = lax.rsqrt(squares[:, None] / width + eps)
    normed = (narrow * scale * norm_gain.astype(jnp.float32)).astype(jnp.bfloat16)
    columns = normed.shape[1]
    flat = expert_ids.reshape(-1)
    onehot = (flat[:, None] == jnp.arange(experts, dtype=jnp.int32)[None, :]).astype(jnp.int32)
    ranking = jnp.sum(jnp.cumsum(onehot, axis=0) * onehot, axis=1) - 1
    target = flat * capacity + ranking
    sources = jnp.arange(tok_dev * top, dtype=jnp.int32) // top
    owner = jnp.full((experts * capacity,), tok_dev, jnp.int32).at[target].set(sources)
    padded = jnp.concatenate([normed, jnp.zeros((1, columns), jnp.bfloat16)], axis=0)
    outgoing = padded[owner].reshape(n_ep, exp_dev * capacity, columns)
    arrived = lax.all_to_all(outgoing, "ep", split_axis=0, concat_axis=0, tiled=True)
    rows = (
        arrived.reshape(n_ep, exp_dev, capacity, columns)
        .transpose(1, 0, 2, 3)
        .reshape(exp_dev, n_ep * capacity, columns)
    )
    piece = lax.all_gather(rows, "tp", axis=2, tiled=True)
    gate = jnp.einsum("erd,edf->erf", piece, w_gate, preferred_element_type=jnp.float32)
    upper = jnp.einsum("erd,edf->erf", piece, w_up, preferred_element_type=jnp.float32)
    hidden = (jax.nn.silu(gate) * upper).astype(jnp.bfloat16)
    partial_out = jnp.einsum(
        "erf,efd->erd", hidden, w_down, preferred_element_type=jnp.float32
    ).astype(jnp.bfloat16)
    shares = (
        lax.psum_scatter(partial_out, "tp", scatter_dimension=2, tiled=True)
        .astype(jnp.float32)
        .astype(jnp.bfloat16)
    )
    homeward = (
        shares.reshape(exp_dev, n_ep, capacity, half)
        .transpose(1, 0, 2, 3)
        .reshape(n_ep, exp_dev * capacity, half)
    )
    returned = lax.all_to_all(homeward, "ep", split_axis=0, concat_axis=0, tiled=True).reshape(
        experts * capacity, half
    )
    picked = returned[target].astype(jnp.float32).reshape(tok_dev, top, half)
    mixed = jnp.sum(picked * combine[:, :, None], axis=1)
    totals = lax.psum(jnp.sum(mixed * mixed, axis=1), "tp")
    norm = lax.rsqrt(totals[:, None] / width + eps)
    return (mixed * norm * final_gain.astype(jnp.float32)).astype(jnp.bfloat16)


def solution(mesh):
    placed = (
        P(("grp", "ep"), "tp"),
        P("tp"),
        P("ep", None, "tp"),
        P("ep", None, "tp"),
        P("ep", "tp", None),
        P(("grp", "ep"), None),
        P(("grp", "ep"), None),
        P("tp"),
    )
    return jax.shard_map(
        body, mesh=mesh, in_specs=placed, out_specs=P(("grp", "ep"), "tp"), check_vma=False
    )
```

profile of v0, /device:TPU:1, one launch (start us, length us, event | category | flops | bytes accessed | tf_op | source)
XLA Modules:
  0.0 224.8 jit_solution(16053872975609984581)
XLA Ops:
  6.5 1.0 copy.11
  7.5 0.1 eq.29
  7.7 0.1 eq.25
  7.8 0.7 broadcast_multiply_fusion
  8.5 1.1 reduce-window.6
  9.6 0.2 slice_reduce_fusion
  9.9 0.1 fusion.21
  10.0 0.1 copy.10
  10.1 0.1 mul.81
  10.3 2.5 %scatter_custom_fusion = s32[1280]{0:T(1024)S(1)} fusion(s32[512]{0:T(512)S(1)} %bitcast.39, s32[512]{0:T(512)S(1)} %add_select_fusion, s32[]{:T(128)} %constant.38.clone.1), kind=kCustom, calls=%fused_computation.35 | custom fusion | bytes 5124 | tf_op jit(solution)/shard_map/scatter | solution.py:30
  12.8 0.7 convert_element_type.40
  13.5 1.2 fusion.18
  14.7 2.5 %psum.14 = f32[256]{0:T(256)S(1)} all-reduce(f32[256]{0:T(256)S(1)} %fusion.18), channel_id=1, replica_groups=mesh['grp'=2,'ep'=8,'tp'=2] {'tp'}, use_global_device_ids=true, to_apply=%region_1.0 | all-reduce | flops 256 | bytes 2048 | tf_op jit(solution)/shard_map/psum | solution.py:21
  17.2 1.2 fusion.20
  18.5 5.1 %gather_fusion = bf16[1280,1024]{1,0:T(8,128)(2,1)} fusion(bf16[257,1024]{1,0:T(8,128)(2,1)S(1)} %concatenate.3, s32[2048]{0:T(1024)S(1)} %pad_clamp_fusion), kind=kCustom, calls=%fused_computation | custom fusion | bytes 5248000 | tf_op jit(solution)/shard_map/gather | solution.py:32
  23.5 65.4 %all_to_all.10 = bf16[8,160,1024]{2,1,0:T(8,128)(2,1)} all-to-all(bf16[8,160,1024]{2,1,0:T(8,128)(2,1)} %bitcast.37), channel_id=1, replica_groups=mesh['grp'=2,'ep'=8,'tp'=2] {'ep'}, dimensions={0} | all-to-all | bytes 5242880 | tf_op jit(solution)/shard_map/all_to_all | solution.py:33
  88.9 0.0 all-gather.2.cloned.1.call-update
  88.9 0.0 reduce-scatter.2.cloned.1.call-start
  89.0 15.9 %all-gather.2.cloned.1.call-done = bf16[1,1280,2048]{2,1,0:T(8,128)(2,1)} async-done(((bf16[1,1280,1024]{2,1,0:T(8,128)(2,1)}), bf16[1,1280,2048]{2,1,0:T(8,128)(2,1)}) %all-gather.2.cloned.1.call-update) | async-done | bytes 5242896 | tf_op jit(solution)/shard_map/all_gather | solution.py:39
  104.9 7.6 %fusion.3 = f32[1280,512]{1,0:T(8,128)} fusion(bf16[1,1280,2048]{2,1,0:T(8,128)(2,1)} %all-gather.2.cloned.1.call-done, bf16[1,2048,512]{2,1,0:T(8,128)(2,1)} %param.10), kind=kOutput, calls=%fused_computation.7 | convolution fusion | flops 2684354560 | bytes 9961472 | tf_op jit(solution)/shard_map/erd,edf->erf/dot_general | solution.py:40
  112.4 10.3 %fusion = bf16[1,1280,2048]{2,1,0:T(8,128)(2,1)} fusion(bf16[1,512,2048]{2,1,0:T(8,128)(2,1)S(1)} %copy-done, bf16[1,1280,2048]{2,1,0:T(8,128)(2,1)} %all-gather.2.cloned.1.call-done, f32[1280,512]{1,0:T(8,128)} %fusion.3, bf16[1,2048,512]{2,1,0:T(8,128)(2,1)} %param.11), kind=kOutput, calls=%fused_computation.4 | convolution fusion | flops 5375262720 | bytes 17301504 | tf_op jit(solution)/shard_map/erf,efd->erd/dot_general | solution.py:43
  122.8 0.0 reduce-scatter.2.cloned.1.call-update
  122.8 14.3 %reduce-scatter.2.cloned.1.call-done = bf16[1,1280,1024]{2,1,0:T(8,128)(2,1)} async-done(((bf16[1,1280,2048]{2,1,0:T(8,128)(2,1)}), bf16[1,1280,1024]{2,1,0:T(8,128)(2,1)}) %reduce-scatter.2.cloned.1.call-update) | async-done | bytes 2621456 | tf_op jit(solution)/shard_map/reduce_scatter | solution.py:47
  137.1 5.6 %all-to-all-start.1 = ((bf16[8,160,1024]{2,1,0:T(8,128)(2,1)}), bf16[8,160,1024]{2,1,0:T(8,128)(2,1)}, u32[]{:S(2)}, u32[]{:S(2)}) async-start(bf16[8,160,1024]{2,1,0:T(8,128)(2,1)} %bitcast.38), calls=%async_computation.2 | async-start | bytes 5242880 | tf_op jit(solution)/shard_map/all_to_all | solution.py:56
  142.7 0.1 copy.13
  142.9 58.9 %all-to-all-done.1 = bf16[8,160,1024]{2,1,0:T(8,128)(2,1)} async-done(((bf16[8,160,1024]{2,1,0:T(8,128)(2,1)}), bf16[8,160,1024]{2,1,0:T(8,128)(2,1)}, u32[]{:S(2)}, u32[]{:S(2)}) %all-to-all-start.1) | async-done | bytes 2621472 | tf_op jit(solution)/shard_map/all_to_all | solution.py:56
  201.8 4.8 %gather_fusion.1 = bf16[512,1024]{1,0:T(8,128)(2,1)S(1)} fusion(bf16[1280,1024]{1,0:T(8,128)(2,1)} %bitcast.12, s32[1024]{0:T(1024)S(1)} %pad_clamp_fusion.1), kind=kCustom, calls=%fused_computation.1 | custom fusion | bytes 2099200 | tf_op jit(solution)/shard_map/gather | solution.py:59
  206.6 2.4 %reshape.105 = f32[256,2,1024]{2,1,0:T(2,128)} reshape(bf16[512,1024]{1,0:T(8,128)(2,1)S(1)} %gather_fusion.1) | data formatting | bytes 3145728 | tf_op jit(solution)/shard_map/convert_element_type | solution.py:59
  209.0 4.3 %multiply_reduce_fusion = f32[256,1024]{1,0:T(8,128)S(1)} fusion(f32[256,2,1024]{2,1,0:T(2,128)} %reshape.105, f32[256,2]{1,0:T(8,128)S(1)} %copy.13), kind=kLoop, calls=%fused_computation.14 | loop fusion | flops 786432 | bytes 3147776 | tf_op jit(solution)/shard_map/reduce_sum | solution.py:60
  213.3 0.1 multiply_reduce_fusion.1
  213.4 3.6 %psum.15 = f32[256]{0:T(256)S(1)} all-reduce(f32[256]{0:T(256)S(1)} %multiply_reduce_fusion.1), channel_id=1, replica_groups=mesh['grp'=2,'ep'=8,'tp'=2] {'tp'}, use_global_device_ids=true, to_apply=%region_9.10 | all-reduce | flops 256 | bytes 2048 | tf_op jit(solution)/shard_map/psum | solution.py:61
  217.0 1.0 multiply_convert_fusion
  (20 shorter events, 0.1 us)
Async XLA Ops:
  6.5 105.9 %copy-start = (bf16[1,512,2048]{2,1,0:T(8,128)(2,1)S(1)}, bf16[1,512,2048]{2,1,0:T(8,128)(2,1)}, u32[]{:S(2)}) copy-start(bf16[1,512,2048]{2,1,0:T(8,128)(2,1)} %param.12) | copy-start | bytes 6291460
  6.5 98.3 %all-gather.2.cloned.1.call-start = ((), (), s32[]{:S(2)}) async-start(), calls=%async_computation.3 | async-start | bytes 7864320 | tf_op jit(solution)/shard_map/all_gather | solution.py:39
  88.9 48.1 %reduce-scatter.2.cloned.1.call-start = ((), (), s32[]{:S(2)}) async-start(), calls=%async_computation.4 | async-start | bytes 7864320 | tf_op jit(solution)/shard_map/reduce_scatter | solution.py:47
  137.1 5.6 %copy-start.1 = (f32[256,2]{0,1:T(2,128)S(1)}, f32[256,2]{0,1:T(2,128)}, u32[]{:S(2)}) copy-start(f32[256,2]{0,1:T(2,128)} %param.14) | copy-start | bytes 6148
  137.1 5.7 %copy-start.2 = (bf16[1024]{0:T(1024)(128)(2,1)S(1)}, bf16[1024]{0:T(1024)(128)(2,1)}, u32[]{:S(2)}) copy-start(bf16[1024]{0:T(1024)(128)(2,1)} %param.15) | copy-start | bytes 6148
  137.1 64.7 %all-to-all-start.1 = ((bf16[8,160,1024]{2,1,0:T(8,128)(2,1)}), bf16[8,160,1024]{2,1,0:T(8,128)(2,1)}, u32[]{:S(2)}, u32[]{:S(2)}) async-start(bf16[8,160,1024]{2,1,0:T(8,128)(2,1)} %bitcast.38), calls=%async_computation.2 | async-start | bytes 5242880 | tf_op jit(solution)/shard_map/all_to_all | solution.py:56
Sparse Core Ops, SparseCore 0:
  89.1 15.7 all-gather.1
  122.9 14.1 reduce-scatter.1
where the time goes:
time: 226 us; the launch traced here: 225 us
  waiting for transfers between devices  89.1 us (39%)
  blocking collectives  71.4 us (32%)
  matrix products  17.9 us (8%)
  local copies, waits for them, and re-layouts  16.6 us (7%)
  between operations  13.5 us (6%)
  other arithmetic  10.6 us (5%)
  starting transfers between devices  5.63 us (2%)
    all_to_all x1, blocking collectives, body(): lax.all_to_all(outgoing, 'ep', split_axis=0, concat_axis=0, tiled=True)  65.4 us
    all_to_all x1, waiting for transfers between devices, body(): lax.all_to_all(homeward, 'ep', split_axis=0, concat_axis=0, tiled=True)  58.9 us
    all_gather x1, waiting for transfers between devices, body(): piece = lax.all_gather(rows, 'tp', axis=2, tiled=True)  15.9 us
    reduce_scatter x1, waiting for transfers between devices, body(): lax.psum_scatter(partial_out, 'tp', scatter_dimension=2, tiled=True)  14.3 us
    dot_general x1, matrix products, body(): jnp.einsum('erf,efd->erd', hidden, w_down, preferred_element_type=jnp.flo...  10.3 us
    dot_general x1, matrix products, body(): jnp.einsum('erd,edf->erf', piece, w_gate, preferred_element_type=jnp.floa...  7.55 us
    all_to_all x1, starting transfers between devices, body(): lax.all_to_all(homeward, 'ep', split_axis=0, concat_axis=0, tiled=True)  5.58 us
    gather x1, local copies, waits for them, and re-layouts, body(): outgoing = padded[owner].reshape(n_ep, exp_dev * capacity, columns)  5.08 us
  transfers between devices with their start and end apart: 3, of which 3 were waited for; matrix products, arithmetic and copies ran while one was open for 0% of the time, Pallas kernels for 0%

commit v1 on v0

--- a/solution.py
+++ b/solution.py
@@ -1,13 +1,20 @@
+import functools
+
 import jax
 import jax.numpy as jnp
 from jax import lax
+from jax.experimental import pallas as pl
+from jax.experimental.pallas import tpu as pltpu
 from jax.sharding import PartitionSpec as P
 
 GROUPS = 4
-
-
-def body(tokens, norm_gain, w_gate, w_up, w_down, expert_ids, combine, final_gain):
-    eps = 1e-06
+EPS = 1e-06
+MESH = pl.DeviceIdType.MESH
+bf16, f32 = jnp.bfloat16, jnp.float32
+
+
+def general(tokens, norm_gain, w_gate, w_up, w_down, expert_ids, combine, final_gain):
+    eps = EPS
     tok_dev, half = tokens.shape
     n_ep = lax.axis_size("ep")
     n_tp = lax.axis_size("tp")
@@ -63,6 +70,242 @@
     return (mixed * norm * final_gain.astype(jnp.float32)).astype(jnp.bfloat16)
 
 
+def fold(v):
+    v = v * v
+    out = v[:, :128]
+    for i in range(1, v.shape[1] // 128):
+        out = out + v[:, i * 128 : (i + 1) * 128]
+    return out
+
+
+def paired_kernel(
+    G, cap, tok_ref, gain_ref, ids_ref, comb_ref, fgain_ref, wg_hbm, wu_hbm, wd_hbm, out_ref,
+    wg, wu, wd, xbuf, sbuf, meta, psend, pown, precv, ebuf, xret, zbuf, ret, sq,
+    wsem, sq_s, sq_r, z_s, z_r, m_s, m_r, x_s, x_r, t_s, t_r, p_s, p_r, e_s, e_r, h_s, h_r,
+):
+    rows, half = tok_ref.shape
+    ep, c = lax.axis_index("ep"), lax.axis_index("tp")
+    g, j = ep // 2, ep % 2
+    other = {"ep": g * 2 + (1 - j)}
+    core = {"tp": 1 - c}
+
+    def plane(d):
+        return {"ep": ((g + d + G) % G) * 2 + j}
+
+    barrier = pltpu.get_barrier_semaphore()
+    for dev in [core, other] + [plane(d) for d in range(1, G)]:
+        pl.semaphore_signal(barrier, inc=1, device_id=dev, device_id_type=MESH)
+
+    loads = []
+    for i, h in enumerate((c, 1 - c)):
+        at = pl.ds(pl.multiple_of(h * half, half), half)
+        loads.append(pltpu.make_async_copy(wg_hbm.at[0, at, :], wg.at[i], wsem.at[i]))
+        loads.append(pltpu.make_async_copy(wu_hbm.at[0, at, :], wu.at[i], wsem.at[2 + i]))
+        loads.append(pltpu.make_async_copy(wd_hbm.at[0, :, at], wd.at[i], wsem.at[4 + i]))
+    for load in loads:
+        load.start()
+
+    sent = []
+
+    def send(src, dst, s, r, dev):
+        copy = pltpu.make_async_remote_copy(
+            src_ref=src, dst_ref=dst, send_sem=s, recv_sem=r, device_id=dev, device_id_type=MESH
+        )
+        copy.start()
+        sent.append(copy)
+        return copy
+
+    x = tok_ref[...].astype(f32)
+    sq[0] = fold(x)
+
+    group = ids_ref[0:1, :] // 2
+    slot8 = lax.broadcasted_iota(jnp.int32, (8, rows), 0)
+    onehot = (slot8 == group).astype(f32)
+    up_to = lax.broadcasted_iota(jnp.int32, (rows, rows), 0) <= lax.broadcasted_iota(
+        jnp.int32, (rows, rows), 1
+    )
+    counted = jnp.dot(onehot.astype(bf16), up_to.astype(f32).astype(bf16), preferred_element_type=f32)
+    rank = jnp.sum(onehot * counted, axis=0, keepdims=True) - 1.0
+    offset = (group - g + G) % G
+    target = offset * cap + rank.astype(jnp.int32)
+    first = ids_ref[0:1, :] % 2 == 0
+    c0, c1 = comb_ref[0:1, :], comb_ref[1:2, :]
+    table = jnp.where(slot8 == 0, jnp.where(first, c0, c1), 0.0)
+    table = jnp.where(slot8 == 1, jnp.where(first, c1, c0), table)
+    table = jnp.where(slot8 == 2, rank, table)
+    table = jnp.where(slot8 == 3, group.astype(f32), table)
+    meta[0] = table
+    pick = (lax.broadcasted_iota(jnp.int32, (G * cap, rows), 0) == target).astype(f32).astype(bf16)
+
+    pl.semaphore_wait(barrier, 1 + G)
+    first_sq = send(sq.at[0], sq.at[1], sq_s.at[0], sq_r.at[0], core)
+    metas = [None] + [
+        send(meta.at[0], meta.at[d], m_s.at[d], m_r.at[d], plane(d)) for d in range(1, G)
+    ]
+    first_sq.wait_recv()
+    total = jnp.sum(sq[0] + sq[1], axis=1, keepdims=True)
+    scale = lax.rsqrt(total / (2 * half) + EPS)
+    normed = (x * scale * gain_ref[...].astype(f32)).astype(bf16)
+
+    def gather(d):
+        return jnp.dot(
+            pick[d * cap : (d + 1) * cap], normed, preferred_element_type=f32
+        ).astype(bf16)
+
+    zs, xs, ts, fs, ps, es, hs = ([None] * G for _ in range(7))
+
+    def arrived(d):
+        if d:
+            zs[d].wait_recv()
+        xs[d] = send(xbuf.at[0, d, 0], xbuf.at[0, d, 1], x_s.at[d], x_r.at[d], other)
+        ts[d] = send(xbuf.at[0, d, 0], xbuf.at[1, d, 0], t_s.at[d, 0], t_r.at[d, 0], core)
+
+    def crossed(d):
+        xs[d].wait_recv()
+        fs[d] = send(xbuf.at[0, d, 1], xbuf.at[1, d, 1], t_s.at[d, 1], t_r.at[d, 1], core)
+
+    def compute(d):
+        ts[d].wait_recv()
+        fs[d].wait_recv()
+        a = xbuf[0, d].reshape(2 * cap, half)
+        b = xbuf[1, d].reshape(2 * cap, half)
+        gate = jnp.dot(a, wg[0], preferred_element_type=f32) + jnp.dot(
+            b, wg[1], preferred_element_type=f32
+        )
+        upper = jnp.dot(a, wu[0], preferred_element_type=f32) + jnp.dot(
+            b, wu[1], preferred_element_type=f32
+        )
+        hidden = (gate / (1.0 + jnp.exp(-gate)) * upper).astype(bf16)
+        psend[d] = jnp.dot(hidden, wd[1], preferred_element_type=f32).astype(bf16).reshape(2, cap, half)
+        ps[d] = send(psend.at[d], precv.at[d], p_s.at[d], p_r.at[d], core)
+        pown[d] = jnp.dot(hidden, wd[0], preferred_element_type=f32).astype(bf16).reshape(2, cap, half)
+
+    def summed(d):
+        ps[d].wait_recv()
+        ebuf[d, 1] = (pown[d, 1].astype(f32) + precv[d, 1].astype(f32)).astype(bf16)
+        es[d] = send(ebuf.at[d, 1], xret.at[d], e_s.at[d], e_r.at[d], other)
+        ebuf[d, 0] = (pown[d, 0].astype(f32) + precv[d, 0].astype(f32)).astype(bf16)
+
+    def mix(d):
+        if d:
+            metas[d].wait_recv()
+        tab = meta[d]
+        slots = lax.broadcasted_iota(jnp.int32, (cap, rows), 0)
+        here = (tab[2:3].astype(jnp.int32) == slots) & (tab[3:4].astype(jnp.int32) == g)
+        mine = jnp.where(j == 0, tab[0:1], tab[1:2])
+        theirs = jnp.where(j == 0, tab[1:2], tab[0:1])
+        mine = jnp.sum(jnp.where(here, mine, 0.0), axis=1, keepdims=True)
+        theirs = jnp.sum(jnp.where(here, theirs, 0.0), axis=1, keepdims=True)
+        es[d].wait_recv()
+        value = (mine * ebuf[d, 0].astype(f32) + theirs * xret[d].astype(f32)).astype(bf16)
+        if d:
+            zbuf[d] = value
+            hs[d] = send(zbuf.at[d], ret.at[d], h_s.at[d], h_r.at[d], plane(-d))
+        else:
+            ret[0] = value
+
+    for d in range(1, G):
+        sbuf[d] = gather(d)
+        zs[d] = send(sbuf.at[d], xbuf.at[0, d, 0], z_s.at[d], z_r.at[d], plane(d))
+        if d == 1:
+            xbuf[0, 0, 0] = gather(0)
+            arrived(0)
+    for load in loads:
+        load.wait()
+    for step in range(G + 1):
+        if step + 1 < G:
+            arrived(step + 1)
+        if step < G:
+            crossed(step)
+            compute(step)
+            summed(step)
+        if step >= 1:
+            mix(step - 1)
+
+    eye = lax.broadcasted_iota(jnp.int32, (rows, rows), 0) == lax.broadcasted_iota(
+        jnp.int32, (rows, rows), 1
+    )
+    back = jnp.sum(jnp.where(eye, target.astype(f32), 0.0), axis=1, keepdims=True).astype(jnp.int32)
+    mixed = jnp.zeros((rows, half), f32)
+    for d in range(G):
+        if d:
+            hs[d].wait_recv()
+        place = lax.broadcasted_iota(jnp.int32, (rows, cap), 1) + d * cap == back
+        mixed = mixed + jnp.dot(
+            place.astype(f32).astype(bf16), ret[d], preferred_element_type=f32
+        )
+    sq[2] = fold(mixed)
+    last_sq = send(sq.at[2], sq.at[3], sq_s.at[1], sq_r.at[1], core)
+    last_sq.wait_recv()
+    total = jnp.sum(sq[2] + sq[3], axis=1, keepdims=True)
+    norm = lax.rsqrt(total / (2 * half) + EPS)
+    out_ref[...] = (mixed * norm * fgain_ref[...].astype(f32)).astype(bf16)
+    for copy in sent:
+        copy.wait_send()
+
+
+def paired(tokens, norm_gain, w_gate, w_up, w_down, expert_ids, combine, final_gain):
+    rows, half = tokens.shape
+    G = lax.axis_size("ep") // 2
+    cap = rows // 8 * 5
+    ff = w_gate.shape[2]
+    vmem = pl.BlockSpec(memory_space=pltpu.VMEM)
+    hbm = pl.BlockSpec(memory_space=pl.ANY)
+    dma = pltpu.SemaphoreType.DMA
+    return pl.pallas_call(
+        functools.partial(paired_kernel, G, cap),
+        out_shape=jax.ShapeDtypeStruct((rows, half), bf16),
+        in_specs=[vmem] * 5 + [hbm] * 3,
+        out_specs=vmem,
+        scratch_shapes=[
+            pltpu.VMEM((2, half, ff), bf16),
+            pltpu.VMEM((2, half, ff), bf16),
+            pltpu.VMEM((2, ff, half), bf16),
+            pltpu.VMEM((2, G, 2, cap, half), bf16),
+            pltpu.VMEM((G, cap, half), bf16),
+            pltpu.VMEM((G, 8, rows), f32),
+            pltpu.VMEM((G, 2, cap, half), bf16),
+            pltpu.VMEM((G, 2, cap, half), bf16),
+            pltpu.VMEM((G, 2, cap, half), bf16),
+            pltpu.VMEM((G, 2, cap, half), bf16),
+            pltpu.VMEM((G, cap, half), bf16),
+            pltpu.VMEM((G, cap, half), bf16),
+            pltpu.VMEM((G, cap, half), bf16),
+            pltpu.VMEM((4, rows, 128), f32),
+            dma((6,)),
+            dma((2,)), dma((2,)),
+            dma((G,)), dma((G,)),
+            dma((G,)), dma((G,)),
+            dma((G,)), dma((G,)),
+            dma((G, 2)), dma((G, 2)),
+            dma((G,)), dma((G,)),
+            dma((G,)), dma((G,)),
+            dma((G,)), dma((G,)),
+        ],
+        compiler_params=pltpu.CompilerParams(
+            collective_id=0, has_side_effects=True, vmem_limit_bytes=60 * 1024 * 1024
+        ),
+        name="paired",
+    )(
+        tokens, norm_gain[None, :], expert_ids.T, combine.T, final_gain[None, :],
+        w_gate, w_up, w_down,
+    )
+
+
+def body(tokens, norm_gain, w_gate, w_up, w_down, expert_ids, combine, final_gain):
+    experts = w_gate.shape[0] * lax.axis_size("ep")
+    per_group = experts // GROUPS
+    args = (tokens, norm_gain, w_gate, w_up, w_down, expert_ids, combine, final_gain)
+    if (
+        per_group == expert_ids.shape[1] == 2
+        and w_gate.shape[0] == 1
+        and lax.axis_size("tp") == 2
+        and GROUPS <= 8
+    ):
+        return paired(*args)
+    return general(*args)
+
+
 def solution(mesh):
     placed = (
         P(("grp", "ep"), "tp"),

time: 226 us -> 92 us (0.41)
  waiting for transfers between devices: 89.1 us -> 0 us
  Pallas kernels: 0 us -> 87.3 us
  blocking collectives: 71.4 us -> 0 us
  matrix products: 17.9 us -> 0 us
  between operations: 13.5 us -> 0.01 us
  local copies, waits for them, and re-layouts: 16.6 us -> 4.42 us
  other arithmetic: 10.6 us -> 0 us
  starting transfers between devices: 5.63 us -> 0 us
    pallas_call x0 -> x1, Pallas kernels: none -> 87.3 us  [paired(): pl.pallas_call(functools.partial(paired_kernel, G, cap), out_shape=jax.Sh...]
    all_to_all x1 -> x0, blocking collectives: 65.4 us -> none  [body(): lax.all_to_all(outgoing, 'ep', split_axis=0, concat_axis=0, tiled=True)]
    all_to_all x1 -> x0, waiting for transfers between devices: 58.9 us -> none  [body(): lax.all_to_all(homeward, 'ep', split_axis=0, concat_axis=0, tiled=True)]
    dot_general x2 -> x0, matrix products: 17.9 us -> none  [the longest x1 10.3 us: body(): jnp.einsum('erf,efd->erd', hidden, w_down, preferred_element_type=jnp.flo...]
    all_gather x1 -> x0, waiting for transfers between devices: 15.9 us -> none  [body(): piece = lax.all_gather(rows, 'tp', axis=2, tiled=True)]
    reduce_scatter x1 -> x0, waiting for transfers between devices: 14.3 us -> none  [body(): lax.psum_scatter(partial_out, 'tp', scatter_dimension=2, tiled=True)]
    gather x2 -> x0, local copies, waits for them, and re-layouts: 9.89 us -> none  [the longest x1 5.08 us: body(): outgoing = padded[owner].reshape(n_ep, exp_dev * capacity, columns)]
    psum x2 -> x0, blocking collectives: 6.03 us -> none  [the longest x1 3.55 us: body(): totals = lax.psum(jnp.sum(mixed * mixed, axis=1), 'tp')]
  transfers between devices with their start and end apart: 3 -> 0, of which waited for: 3 -> 0; matrix products, arithmetic and copies ran while one was open for 0% -> 0% of each run, Pallas kernels for 0% -> 0%
where the time goes in v1:
time: 92 us; the launch traced here: 91.8 us
  Pallas kernels  87.3 us (95%)
  local copies, waits for them, and re-layouts  4.42 us (5%)
    pallas_call x1, Pallas kernels, paired(): pl.pallas_call(functools.partial(paired_kernel, G, cap), out_shape=jax.Sh...  87.3 us
    unnamed x1, local copies, waits for them, and re-layouts  1.87 us

profile of v1, /device:TPU:1, one launch (start us, length us, event | category | flops | bytes accessed | tf_op | source)
XLA Modules:
  0.0 91.8 jit_solution(6137373011356052157)
XLA Ops:
  0.0 1.3 %broadcast_in_dim.6.gain_ref = bf16[1,1024]{1,0:T(2,128)(2,1)} reshape(bf16[1024]{0:T(1024)(128)(2,1)} %param.9) | data formatting | bytes 4096 | tf_op jit(solution)/shard_map/broadcast_in_dim | solution.py:290
  1.3 1.3 %broadcast_in_dim.7.fgain_ref = bf16[1,1024]{1,0:T(2,128)(2,1)} reshape(bf16[1024]{0:T(1024)(128)(2,1)} %param.15) | data formatting | bytes 4096 | tf_op jit(solution)/shard_map/broadcast_in_dim | solution.py:290
  2.6 87.3 %paired.1 = bf16[256,1024]{1,0:T(8,128)(2,1)} custom-call(bf16[256,1024]{1,0:T(8,128)(2,1)} %tok_ref.1, bf16[1,1024]{1,0:T(2,128)(2,1)} %broadcast_in_dim.6.gain_ref, s32[2,256]{1,0:T(2,128)} %bitcast.2, f32[2,256]{1,0:T(2,128)} %bitcast.3, bf16[1,1024]{1,0:T(2,128)(2,1)} %broadcast_in_dim.7.fgain_ref, bf16[1,2048,512]{2,1,0:T(8,128)(2,1)} %wg_hbm.1, ...), custom_call_target="tpu_custom_call" | custom-call | tf_op jit(solution)/shard_map/paired/pallas_call | solution.py:255
  89.9 1.9 %copy.10 = bf16[256,1024]{1,0:T(8,128)(2,1)} copy(bf16[256,1024]{1,0:T(8,128)(2,1)} %paired.1) | data formatting | bytes 1048576

commit v2 on v1

--- a/solution.py
+++ b/solution.py
@@ -9,6 +9,7 @@
 
 GROUPS = 4
 EPS = 1e-06
+LEAD = 1
 MESH = pl.DeviceIdType.MESH
 bf16, f32 = jnp.bfloat16, jnp.float32
 
@@ -79,7 +80,7 @@
 
 
 def paired_kernel(
-    G, cap, tok_ref, gain_ref, ids_ref, comb_ref, fgain_ref, wg_hbm, wu_hbm, wd_hbm, out_ref,
+    G, cap, tok_ref, gain_ref, ids_ref, comb_ref, wg_hbm, wu_hbm, wd_hbm, out_ref,
     wg, wu, wd, xbuf, sbuf, meta, psend, pown, precv, ebuf, xret, zbuf, ret, sq,
     wsem, sq_s, sq_r, z_s, z_r, m_s, m_r, x_s, x_r, t_s, t_r, p_s, p_r, e_s, e_r, h_s, h_r,
 ):
@@ -89,8 +90,16 @@
     other = {"ep": g * 2 + (1 - j)}
     core = {"tp": 1 - c}
 
+    cut = cap // 2
+
+    def flip(a, d):
+        return (a % 2 + d % 2) % 2 + 2 * ((a // 2 + d // 2) % 2)
+
     def plane(d):
-        return {"ep": ((g + d + G) % G) * 2 + j}
+        return {"ep": flip(g, d) * 2 + j}
+
+    inner = ((g + 1) // 2) % 2
+    order = [0, 1, 2 + inner, 3 - inner]
 
     barrier = pltpu.get_barrier_semaphore()
     for dev in [core, other] + [plane(d) for d in range(1, G)]:
@@ -126,7 +135,7 @@
     )
     counted = jnp.dot(onehot.astype(bf16), up_to.astype(f32).astype(bf16), preferred_element_type=f32)
     rank = jnp.sum(onehot * counted, axis=0, keepdims=True) - 1.0
-    offset = (group - g + G) % G
+    offset = flip(group, g)
     target = offset * cap + rank.astype(jnp.int32)
     first = ids_ref[0:1, :] % 2 == 0
     c0, c1 = comb_ref[0:1, :], comb_ref[1:2, :]
@@ -140,35 +149,43 @@
     pl.semaphore_wait(barrier, 1 + G)
     first_sq = send(sq.at[0], sq.at[1], sq_s.at[0], sq_r.at[0], core)
     metas = [None] + [
-        send(meta.at[0], meta.at[d], m_s.at[d], m_r.at[d], plane(d)) for d in range(1, G)
+        send(meta.at[0], meta.at[d], m_s.at[d], m_r.at[d], plane(d)) for d in order[1:]
     ]
     first_sq.wait_recv()
     total = jnp.sum(sq[0] + sq[1], axis=1, keepdims=True)
     scale = lax.rsqrt(total / (2 * half) + EPS)
-    normed = (x * scale * gain_ref[...].astype(f32)).astype(bf16)
+    normed = (x * scale * gain_ref[...].astype(f32)[None, :]).astype(bf16)
 
     def gather(d):
         return jnp.dot(
             pick[d * cap : (d + 1) * cap], normed, preferred_element_type=f32
         ).astype(bf16)
 
-    zs, xs, ts, fs, ps, es, hs = ([None] * G for _ in range(7))
-
-    def arrived(d):
-        if d:
-            zs[d].wait_recv()
-        xs[d] = send(xbuf.at[0, d, 0], xbuf.at[0, d, 1], x_s.at[d], x_r.at[d], other)
-        ts[d] = send(xbuf.at[0, d, 0], xbuf.at[1, d, 0], t_s.at[d, 0], t_r.at[d, 0], core)
-
-    def crossed(d):
-        xs[d].wait_recv()
-        fs[d] = send(xbuf.at[0, d, 1], xbuf.at[1, d, 1], t_s.at[d, 1], t_r.at[d, 1], core)
-
-    def compute(d):
-        ts[d].wait_recv()
-        fs[d].wait_recv()
-        a = xbuf[0, d].reshape(2 * cap, half)
-        b = xbuf[1, d].reshape(2 * cap, half)
+    units = [(d, r) for d in order for r in range(2)]
+    U = len(units)
+    zs, xs, ts, fs, ps, es, hs = ([None] * U for _ in range(7))
+
+    def arrived(u):
+        d, r = units[u]
+        if zs[u] is not None:
+            zs[u].wait_recv()
+        mine = xbuf.at[0, d, r, 0]
+        xs[u] = send(mine, xbuf.at[0, d, r, 1], x_s.at[d, r], x_r.at[d, r], other)
+        ts[u] = send(mine, xbuf.at[1, d, r, 0], t_s.at[d, r, 0], t_r.at[d, r, 0], core)
+
+    def crossed(u):
+        d, r = units[u]
+        xs[u].wait_recv()
+        fs[u] = send(
+            xbuf.at[0, d, r, 1], xbuf.at[1, d, r, 1], t_s.at[d, r, 1], t_r.at[d, r, 1], core
+        )
+
+    def compute(u):
+        d, r = units[u]
+        ts[u].wait_recv()
+        fs[u].wait_recv()
+        a = xbuf[0, d, r].reshape(2 * cut, half)
+        b = xbuf[1, d, r].reshape(2 * cut, half)
         gate = jnp.dot(a, wg[0], preferred_element_type=f32) + jnp.dot(
             b, wg[1], preferred_element_type=f32
         )
@@ -176,70 +193,85 @@
             b, wu[1], preferred_element_type=f32
         )
         hidden = (gate / (1.0 + jnp.exp(-gate)) * upper).astype(bf16)
-        psend[d] = jnp.dot(hidden, wd[1], preferred_element_type=f32).astype(bf16).reshape(2, cap, half)
-        ps[d] = send(psend.at[d], precv.at[d], p_s.at[d], p_r.at[d], core)
-        pown[d] = jnp.dot(hidden, wd[0], preferred_element_type=f32).astype(bf16).reshape(2, cap, half)
-
-    def summed(d):
-        ps[d].wait_recv()
-        ebuf[d, 1] = (pown[d, 1].astype(f32) + precv[d, 1].astype(f32)).astype(bf16)
-        es[d] = send(ebuf.at[d, 1], xret.at[d], e_s.at[d], e_r.at[d], other)
-        ebuf[d, 0] = (pown[d, 0].astype(f32) + precv[d, 0].astype(f32)).astype(bf16)
-
-    def mix(d):
-        if d:
-            metas[d].wait_recv()
+        away = jnp.dot(hidden, wd[1], preferred_element_type=f32)
+        psend[d, r] = away.astype(bf16).reshape(2, cut, half)
+        ps[u] = send(psend.at[d, r], precv.at[d, r], p_s.at[d, r], p_r.at[d, r], core)
+        home = jnp.dot(hidden, wd[0], preferred_element_type=f32)
+        pown[d, r] = home.astype(bf16).reshape(2, cut, half)
+
+    def summed(u):
+        d, r = units[u]
+        ps[u].wait_recv()
+        ebuf[d, r, 1] = (pown[d, r, 1].astype(f32) + precv[d, r, 1].astype(f32)).astype(bf16)
+        es[u] = send(ebuf.at[d, r, 1], xret.at[d, r], e_s.at[d, r], e_r.at[d, r], other)
+        ebuf[d, r, 0] = (pown[d, r, 0].astype(f32) + precv[d, r, 0].astype(f32)).astype(bf16)
+
+    def mix(u):
+        d, r = units[u]
+        if u >= 2 and r == 0:
+            metas[u // 2].wait_recv()
         tab = meta[d]
-        slots = lax.broadcasted_iota(jnp.int32, (cap, rows), 0)
+        slots = lax.broadcasted_iota(jnp.int32, (cut, rows), 0) + r * cut
         here = (tab[2:3].astype(jnp.int32) == slots) & (tab[3:4].astype(jnp.int32) == g)
         mine = jnp.where(j == 0, tab[0:1], tab[1:2])
         theirs = jnp.where(j == 0, tab[1:2], tab[0:1])
         mine = jnp.sum(jnp.where(here, mine, 0.0), axis=1, keepdims=True)
         theirs = jnp.sum(jnp.where(here, theirs, 0.0), axis=1, keepdims=True)
-        es[d].wait_recv()
-        value = (mine * ebuf[d, 0].astype(f32) + theirs * xret[d].astype(f32)).astype(bf16)
-        if d:
-            zbuf[d] = value
-            hs[d] = send(zbuf.at[d], ret.at[d], h_s.at[d], h_r.at[d], plane(-d))
+        es[u].wait_recv()
+        value = (mine * ebuf[d, r, 0].astype(f32) + theirs * xret[d, r].astype(f32)).astype(bf16)
+        if u >= 2:
+            zbuf[d, r] = value
+            hs[u] = send(zbuf.at[d, r], ret.at[d, r], h_s.at[d, r], h_r.at[d, r], plane(d))
         else:
-            ret[0] = value
-
-    for d in range(1, G):
-        sbuf[d] = gather(d)
-        zs[d] = send(sbuf.at[d], xbuf.at[0, d, 0], z_s.at[d], z_r.at[d], plane(d))
-        if d == 1:
-            xbuf[0, 0, 0] = gather(0)
-            arrived(0)
+            ret[0, r] = value
+
+    def depart(u):
+        d, r = units[u]
+        zs[u] = send(sbuf.at[d, r], xbuf.at[0, d, r, 0], z_s.at[d, r], z_r.at[d, r], plane(d))
+
+    sbuf[1] = gather(1).reshape(2, cut, half)
+    depart(2)
+    depart(3)
+    own = gather(0).reshape(2, cut, half)
+    for r in range(2):
+        xbuf[0, 0, r, 0] = own[r]
+        arrived(r)
+    for d in range(2, G):
+        sbuf[d] = gather(d).reshape(2, cut, half)
+    for u in range(4, U):
+        depart(u)
     for load in loads:
         load.wait()
-    for step in range(G + 1):
-        if step + 1 < G:
-            arrived(step + 1)
-        if step < G:
-            crossed(step)
-            compute(step)
-            summed(step)
-        if step >= 1:
-            mix(step - 1)
+    done = 2
+    for u in range(U):
+        while done < min(U, u + LEAD + 1):
+            arrived(done)
+            done += 1
+        crossed(u)
+        compute(u)
+        summed(u)
+        if u:
+            mix(u - 1)
+    mix(U - 1)
 
     eye = lax.broadcasted_iota(jnp.int32, (rows, rows), 0) == lax.broadcasted_iota(
         jnp.int32, (rows, rows), 1
     )
     back = jnp.sum(jnp.where(eye, target.astype(f32), 0.0), axis=1, keepdims=True).astype(jnp.int32)
+    for copy in hs[2:]:
+        copy.wait_recv()
     mixed = jnp.zeros((rows, half), f32)
     for d in range(G):
-        if d:
-            hs[d].wait_recv()
         place = lax.broadcasted_iota(jnp.int32, (rows, cap), 1) + d * cap == back
         mixed = mixed + jnp.dot(
-            place.astype(f32).astype(bf16), ret[d], preferred_element_type=f32
+            place.astype(f32).astype(bf16), ret[d].reshape(cap, half), preferred_element_type=f32
         )
     sq[2] = fold(mixed)
     last_sq = send(sq.at[2], sq.at[3], sq_s.at[1], sq_r.at[1], core)
     last_sq.wait_recv()
     total = jnp.sum(sq[2] + sq[3], axis=1, keepdims=True)
     norm = lax.rsqrt(total / (2 * half) + EPS)
-    out_ref[...] = (mixed * norm * fgain_ref[...].astype(f32)).astype(bf16)
+    out_ref[...] = mixed * norm
     for copy in sent:
         copy.wait_send()
 
@@ -252,44 +284,44 @@
     vmem = pl.BlockSpec(memory_space=pltpu.VMEM)
     hbm = pl.BlockSpec(memory_space=pl.ANY)
     dma = pltpu.SemaphoreType.DMA
-    return pl.pallas_call(
+    out = pl.pallas_call(
         functools.partial(paired_kernel, G, cap),
-        out_shape=jax.ShapeDtypeStruct((rows, half), bf16),
-        in_specs=[vmem] * 5 + [hbm] * 3,
+        out_shape=jax.ShapeDtypeStruct((rows, half), f32),
+        in_specs=[vmem] * 4 + [hbm] * 3,
         out_specs=vmem,
         scratch_shapes=[
             pltpu.VMEM((2, half, ff), bf16),
             pltpu.VMEM((2, half, ff), bf16),
             pltpu.VMEM((2, ff, half), bf16),
-            pltpu.VMEM((2, G, 2, cap, half), bf16),
-            pltpu.VMEM((G, cap, half), bf16),
+            pltpu.VMEM((2, G, 2, 2, cap // 2, half), bf16),
+            pltpu.VMEM((G, 2, cap // 2, half), bf16),
             pltpu.VMEM((G, 8, rows), f32),
-            pltpu.VMEM((G, 2, cap, half), bf16),
-            pltpu.VMEM((G, 2, cap, half), bf16),
-            pltpu.VMEM((G, 2, cap, half), bf16),
-            pltpu.VMEM((G, 2, cap, half), bf16),
-            pltpu.VMEM((G, cap, half), bf16),
-            pltpu.VMEM((G, cap, half), bf16),
-            pltpu.VMEM((G, cap, half), bf16),
+            pltpu.VMEM((G, 2, 2, cap // 2, half), bf16),
+            pltpu.VMEM((G, 2, 2, cap // 2, half), bf16),
+            pltpu.VMEM((G, 2, 2, cap // 2, half), bf16),
+            pltpu.VMEM((G, 2, 2, cap // 2, half), bf16),
+            pltpu.VMEM((G, 2, cap // 2, half), bf16),
+            pltpu.VMEM((G, 2, cap // 2, half), bf16),
+            pltpu.VMEM((G, 2, cap // 2, half), bf16),
             pltpu.VMEM((4, rows, 128), f32),
             dma((6,)),
             dma((2,)), dma((2,)),
+            dma((G, 2)), dma((G, 2)),
             dma((G,)), dma((G,)),
-            dma((G,)), dma((G,)),
-            dma((G,)), dma((G,)),
-            dma((G, 2)), dma((G, 2)),
-            dma((G,)), dma((G,)),
-            dma((G,)), dma((G,)),
-            dma((G,)), dma((G,)),
+            dma((G, 2)), dma((G, 2)),
+            dma((G, 2, 2)), dma((G, 2, 2)),
+            dma((G, 2)), dma((G, 2)),
+            dma((G, 2)), dma((G, 2)),
+            dma((G, 2)), dma((G, 2)),
         ],
         compiler_params=pltpu.CompilerParams(
             collective_id=0, has_side_effects=True, vmem_limit_bytes=60 * 1024 * 1024
         ),
         name="paired",
     )(
-        tokens, norm_gain[None, :], expert_ids.T, combine.T, final_gain[None, :],
-        w_gate, w_up, w_down,
-    )
+        tokens, norm_gain, expert_ids.T, combine.T, w_gate, w_up, w_down,
+    )
+    return (out * final_gain.astype(f32)).astype(bf16)
 
 
 def body(tokens, norm_gain, w_gate, w_up, w_down, expert_ids, combine, final_gain):
@@ -300,7 +332,8 @@
         per_group == expert_ids.shape[1] == 2
         and w_gate.shape[0] == 1
         and lax.axis_size("tp") == 2
-        and GROUPS <= 8
+        and GROUPS == 4
+        and tokens.shape[0] % 256 == 0
     ):
         return paired(*args)
     return general(*args)

time: 92 us -> 87.5 us (0.951)
  local copies, waits for them, and re-layouts: 4.42 us -> 0 us
  other arithmetic: 0 us -> 2.8 us
  Pallas kernels: 87.3 us -> 84.5 us
    pallas_call x1, Pallas kernels: 87.3 us -> 84.5 us  [paired(): pl.pallas_call(functools.partial(paired_kernel, G, cap), out_shape=jax.Sh...]
    convert_element_type x0 -> x2, other arithmetic: none -> 2.8 us  [paired(): return (out * final_gain.astype(f32)).astype(bf16)]
    broadcast_in_dim x2 -> x0, local copies, waits for them, and re-layouts: 2.55 us -> none  [the longest x1 1.28 us: paired(): norm_gain[None, :]]
    unnamed x1 -> x0, local copies, waits for them, and re-layouts: 1.87 us -> none
where the time goes in v2:
time: 87.5 us; the launch traced here: 87.3 us
  Pallas kernels  84.5 us (97%)
  other arithmetic  2.8 us (3%)
    pallas_call x1, Pallas kernels, paired(): pl.pallas_call(functools.partial(paired_kernel, G, cap), out_shape=jax.Sh...  84.5 us
    convert_element_type x2, other arithmetic, paired(): return (out * final_gain.astype(f32)).astype(bf16)  2.8 us

profile of v2, /device:TPU:1, one launch (start us, length us, event | category | flops | bytes accessed | tf_op | source)
XLA Modules:
  0.0 87.3 jit_solution(17139981462789306690)
XLA Ops:
  0.0 0.7 convert_element_type.6
  0.7 84.5 %paired.1 = f32[256,1024]{1,0:T(8,128)} custom-call(bf16[256,1024]{1,0:T(8,128)(2,1)} %tok_ref.1, bf16[1024]{0:T(1024)(128)(2,1)} %gain_ref.1, s32[2,256]{1,0:T(2,128)} %bitcast.2, f32[2,256]{1,0:T(2,128)} %bitcast.3, bf16[1,2048,512]{2,1,0:T(8,128)(2,1)} %wg_hbm.1, bf16[1,2048,512]{2,1,0:T(8,128)(2,1)} %wu_hbm.1, bf16[1,512,2048]{2,1,0:T(8,128)(2,1)} %wd_hbm.1), custom_call_target="tpu_custom_call" | custom-call | tf_op jit(solution)/shard_map/paired/pallas_call | solution.py:287
  85.2 2.1 %multiply_convert_fusion = bf16[256,1024]{1,0:T(8,128)(2,1)} fusion(f32[256,1024]{1,0:T(8,128)} %paired.1, f32[1024]{0:T(1024)S(1)} %convert_element_type.6), kind=kLoop, calls=%fused_computation | loop fusion | flops 524288 | bytes 1576960 | tf_op jit(solution)/shard_map/convert_element_type | solution.py:324
